TPU v7x, 32 devices: a whole 2x2x4 slice. The times are simulated.
32 devices in a mesh: grp: 2 (over x), ep: 4 (over y, core), tp: 4 (over z).
Axes of the slice: x: 2, y: 2, z: 4, core: 2. Of those that a mesh axis runs over, the one named last changes fastest.
Arguments:
- tokens: bfloat16 [3072, 4096], P(('grp', 'ep'), 'tp'), parts along dimension 0
- pre_gain: float32 [4096], replicated, may hold values from 0.1 to 1.9
- out_gain: float32 [4096], P('tp'), may hold values from 0.1 to 1.9
- chosen: int32 [8, 4, 48], P(('grp', 'ep')), parts along dimension 0, may hold values from 0 to 383, as said below
- route_weight: float32 [8, 4, 48], P(('grp', 'ep')), parts along dimension 0, may hold values from 0.3 to 3
- expert_gate: bfloat16 [4, 4096, 3072], P('ep', None, 'tp'), may hold values from -0.09375 to 0.09375
- expert_up: bfloat16 [4, 4096, 3072], P('ep', None, 'tp'), may hold values from -0.09375 to 0.09375
- expert_down: bfloat16 [4, 3072, 4096], P('ep', 'tp'), may hold values from -0.109375 to 0.109375
Outputs:
- output: bfloat16 [3072, 4096], P(('grp', 'ep'), 'tp'), parts along dimension 0
There are 2 independent parts, one for each index of `grp`. A program takes and returns all parts, laid end to end along the dimension named above; an argument that names none is the same for every part. Nothing has to cross between parts.
Inputs may be any that keep to these rules, and one draw needn't show every extreme that they name: chosen[b, e, k] is the position, within block b of 384 tokens, of the k-th token that expert e takes from that block; the 48 positions of one block and one expert are all different.
All inputs are finite; a program needn't handle non-finite values.
Results may differ from a plain program's by a relative error of at most 0.0075.
Values may be sent and summed in bfloat16 or wider, within the bound.
No kernel may reach another device: no remote copies, remote signals or barrier semaphores. Data moves between devices by JAX's collectives and lax.ppermute only.
A program may use at most 64 MiB of HBM per device.

v0:
```python
import jax
import jax.numpy as jnp
from jax import lax
from jax.sharding import PartitionSpec as P

NORM_EPS = 1e-06


def shards(tokens, pre_gain, out_gain, chosen, route_weight, expert_gate, expert_up, expert_down):
    model_width = pre_gain.shape[0]
    shard_width = tokens.shape[1]
    tok_count = tokens.shape[0]
    chosen_here = chosen[0]
    experts_all = chosen_here.shape[0]
    slot_count = chosen_here.shape[1]
    resident = tokens.astype(jnp.float32)
    square_sum = lax.psum(jnp.sum(resident * resident, axis=1), "tp")
    row_scale = lax.rsqrt(square_sum / model_width + NORM_EPS)[:, None]
    gain_slice = lax.dynamic_slice_in_dim(
        pre_gain, lax.axis_index("tp") * shard_width, shard_width, 0
    )
    normed = (resident * row_scale * gain_slice).astype(jnp.bfloat16)
    outgoing = jnp.take(normed, chosen_here, axis=0)
    incoming = lax.all_to_all(outgoing, "ep", split_axis=0, concat_axis=0, tiled=True)
    picked_rows = lax.all_gather(incoming.reshape(-1, shard_width), "tp", axis=1, tiled=True)
    gate_act = jnp.dot(picked_rows, expert_gate[0], preferred_element_type=jnp.float32)
    up_act = jnp.dot(picked_rows, expert_up[0], preferred_element_type=jnp.float32)
    hidden = (jax.nn.silu(gate_act) * up_act).astype(jnp.bfloat16)
    down_shard = expert_down[0]
    summed = lax.psum_scatter(
        lax.dot_general(
            down_shard, hidden, (((0,), (1,)), ((), ())), preferred_element_type=jnp.float32
        ).astype(jnp.bfloat16),
        "tp",
        scatter_dimension=0,
        tiled=True,
    )
    expert_out = summed.reshape(shard_width, experts_all, slot_count)
    returned = lax.all_to_all(expert_out, "ep", split_axis=1, concat_axis=1, tiled=True)
    weighted = returned.astype(jnp.float32) * route_weight[0][None]
    flat_weighted = weighted.reshape(shard_width, experts_all * slot_count)
    update_cols = (
        jnp.zeros((shard_width, tok_count), jnp.float32)
        .at[:, chosen_here.reshape(-1)]
        .add(flat_weighted)
    )
    mixed_rows = resident + update_cols.T
    out_sum = lax.psum(jnp.sum(mixed_rows * mixed_rows, axis=1), "tp")
    out_scale = lax.rsqrt(out_sum / model_width + NORM_EPS)[:, None]
    return (mixed_rows * out_scale * out_gain).astype(jnp.bfloat16)


def solution(mesh):
    return jax.shard_map(
        shards,
        mesh=mesh,
        in_specs=(
            P(("grp", "ep"), "tp"),
            P(),
            P("tp"),
            P(("grp", "ep"), None, None),
            P(("grp", "ep"), None, None),
            P("ep", None, "tp"),
            P("ep", None, "tp"),
            P("ep", "tp", None),
        ),
        out_specs=P(("grp", "ep"), "tp"),
        check_vma=False,
    )
```

profile of v0, /device:TPU:0, one launch (start us, length us, event | category | flops | bytes accessed | tf_op | source)
XLA Modules:
  0.0 150.9 jit_solution(1247583569600255627)
XLA Ops:
  6.5 0.0 all-gather.2.cloned.1.call-start
  6.5 0.7 compare_select_fusion.1
  7.2 0.7 compare_and_fusion
  7.9 1.4 fusion.12
  9.3 13.5 %psum.14 = f32[384]{0:T(512)S(1)} all-reduce(f32[384]{0:T(512)S(1)} %fusion.12), channel_id=1, replica_groups=mesh['grp'=2,'ep'=4,'tp'=4] {'tp'}, use_global_device_ids=true, to_apply=%region_1.0 | all-reduce | flops 384 | bytes 3072 | tf_op jit(solution)/shard_map/psum | solution.py:17
  22.8 0.1 reshape.80
  22.9 0.7 dynamic_slice.3
  23.6 1.4 fusion.14
  24.9 1.0 gather_fusion
  26.0 0.1 broadcast_select_fusion
  26.1 10.5 %all_to_all.10 = bf16[4,48,1024]{2,1,0:T(8,128)(2,1)} all-to-all(bf16[4,48,1024]{2,1,0:T(8,128)(2,1)S(1)} %broadcast_select_fusion), channel_id=1, replica_groups=mesh['grp'=2,'ep'=4,'tp'=4] {'ep'}, dimensions={0} | all-to-all | bytes 786432 | tf_op jit(solution)/shard_map/all_to_all | solution.py:24
  36.5 0.0 all-gather.2.cloned.1.call-update
  36.6 0.0 reduce-scatter.2.cloned.1.call-start
  36.6 34.4 %all-gather.2.cloned.1.call-done = bf16[192,4096]{1,0:T(8,128)(2,1)} async-done(((bf16[192,1024]{1,0:T(8,128)(2,1)}), bf16[192,4096]{1,0:T(8,128)(2,1)}) %all-gather.2.cloned.1.call-update) | async-done | bytes 1572880 | tf_op jit(solution)/shard_map/all_gather | solution.py:25
  71.0 0.0 copy-start.4
  71.0 4.8 %fusion.4 = f32[192,768]{1,0:T(8,128)S(1)} fusion(bf16[192,4096]{1,0:T(8,128)(2,1)} %all-gather.2.cloned.1.call-done, bf16[1,4096,768]{2,1,0:T(8,128)(2,1)} %param.13), kind=kOutput, calls=%fused_computation.6 | convolution fusion | flops 1207959552 | bytes 8454144 | tf_op jit(solution)/shard_map/dot_general | solution.py:26
  75.8 0.0 copy-done.4
  75.8 9.3 %fusion.9 = bf16[4096,192]{0,1:T(8,128)(2,1)} fusion(bf16[1,768,4096]{2,1,0:T(8,128)(2,1)} %param.15, bf16[192,4096]{1,0:T(8,128)(2,1)S(1)} %copy-done.4, bf16[1,4096,768]{2,1,0:T(8,128)(2,1)} %param.14, f32[192,768]{1,0:T(8,128)S(1)} %fusion.4), kind=kOutput, calls=%fused_computation.9 | convolution fusion | flops 2417590272 | bytes 16318464 | tf_op jit(solution)/shard_map/dot_general | solution.py:31
  85.0 0.0 copy-start.1
  85.0 0.0 copy-start.3
  85.0 0.0 reduce-scatter.2.cloned.1.call-update
  85.1 34.4 %reduce-scatter.2.cloned.1.call-done = bf16[1024,192]{0,1:T(8,128)(2,1)} async-done(((bf16[4096,192]{0,1:T(8,128)(2,1)}), bf16[1024,192]{0,1:T(8,128)(2,1)}) %reduce-scatter.2.cloned.1.call-update) | async-done | bytes 393232 | tf_op jit(solution)/shard_map/reduce_scatter | solution.py:30
  119.5 3.5 %all-to-all-start.1 = ((bf16[1024,4,48]{0,2,1:T(8,128)(2,1)}), bf16[1024,4,48]{0,2,1:T(8,128)(2,1)S(1)}, u32[]{:S(2)}, u32[]{:S(2)}) async-start(bf16[1024,4,48]{0,2,1:T(8,128)(2,1)} %bitcast.48), calls=%async_computation.2 | async-start | bytes 786432 | tf_op jit(solution)/shard_map/all_to_all | solution.py:39
  123.0 0.0 copy-done.1
  123.0 0.0 copy-start
  123.0 0.1 reshape_squeeze.3
  123.1 7.3 %all-to-all-done.1 = bf16[1024,4,48]{0,2,1:T(8,128)(2,1)S(1)} async-done(((bf16[1024,4,48]{0,2,1:T(8,128)(2,1)}), bf16[1024,4,48]{0,2,1:T(8,128)(2,1)S(1)}, u32[]{:S(2)}, u32[]{:S(2)}) %all-to-all-start.1) | async-done | bytes 393248 | tf_op jit(solution)/shard_map/all_to_all | solution.py:39
  130.3 0.0 copy-done.3
  130.3 0.1 convert_multiply_fusion.2
  130.5 2.5 %scatter_custom_fusion = f32[1024,384]{0,1:T(8,128)S(1)} fusion(s32[192]{0:T(256)S(1)} %bitcast.50, f32[192,1024]{1,0:T(8,128)S(1)} %bitcast.47, f32[]{:T(128)} %constant.11.clone.1), kind=kCustom, calls=%fused_computation.21 | custom fusion | flops 196608 | bytes 1572868 | tf_op jit(solution)/shard_map/scatter-add | solution.py:45
  133.0 0.0 copy-done
  133.0 0.0 copy-start.2
  133.0 0.3 multiply_reduce_fusion
  133.3 9.6 %psum.15 = f32[384]{0:T(512)S(1)} all-reduce(f32[384]{0:T(512)S(1)} %multiply_reduce_fusion), channel_id=1, replica_groups=mesh['grp'=2,'ep'=4,'tp'=4] {'tp'}, use_global_device_ids=true, to_apply=%region_5.6 | all-reduce | flops 384 | bytes 3072 | tf_op jit(solution)/shard_map/psum | solution.py:48
  142.9 0.0 copy-done.2
  142.9 1.1 multiply_convert_fusion
  (4 shorter events, 0.0 us)
Async XLA Ops:
  6.5 64.5 %all-gather.2.cloned.1.call-start = ((), (), s32[]{:S(2)}) async-start(), calls=%async_computation.3 | async-start | bytes 1966080 | tf_op jit(solution)/shard_map/all_gather | solution.py:25
  36.6 82.9 %reduce-scatter.2.cloned.1.call-start = ((), (), s32[]{:S(2)}) async-start(), calls=%async_computation.4 | async-start | bytes 1966080 | tf_op jit(solution)/shard_map/reduce_scatter | solution.py:30
  71.0 4.8 %copy-start.4 = (bf16[192,4096]{1,0:T(8,128)(2,1)S(1)}, bf16[192,4096]{1,0:T(8,128)(2,1)}, u32[]{:S(2)}) copy-start(bf16[192,4096]{1,0:T(8,128)(2,1)} %all-gather.2.cloned.1.call-done) | copy-start | bytes 4718596
  85.0 37.9 %copy-start.1 = (s32[1,4,48]{2,1,0:T(4,128)S(1)}, s32[1,4,48]{2,1,0:T(4,128)}, u32[]{:S(2)}) copy-start(s32[1,4,48]{2,1,0:T(4,128)} %param.11) | copy-start | bytes 2308
  85.0 45.3 %copy-start.3 = (f32[1,4,48]{2,1,0:T(4,128)S(1)}, f32[1,4,48]{2,1,0:T(4,128)}, u32[]{:S(2)}) copy-start(f32[1,4,48]{2,1,0:T(4,128)} %param.12) | copy-start | bytes 2308
  119.5 10.8 %all-to-all-start.1 = ((bf16[1024,4,48]{0,2,1:T(8,128)(2,1)}), bf16[1024,4,48]{0,2,1:T(8,128)(2,1)S(1)}, u32[]{:S(2)}, u32[]{:S(2)}) async-start(bf16[1024,4,48]{0,2,1:T(8,128)(2,1)} %bitcast.48), calls=%async_computation.2 | async-start | bytes 786432 | tf_op jit(solution)/shard_map/all_to_all | solution.py:39
  123.0 10.0 %copy-start = (bf16[384,1024]{1,0:T(8,128)(2,1)S(1)}, bf16[384,1024]{1,0:T(8,128)(2,1)}, u32[]{:S(2)}) copy-start(bf16[384,1024]{1,0:T(8,128)(2,1)} %param.8) | copy-start | bytes 2359300
  133.0 9.9 %copy-start.2 = (f32[1024]{0:T(1024)S(1)}, f32[1024]{0:T(1024)}, u32[]{:S(2)}) copy-start(f32[1024]{0:T(1024)} %param.10) | copy-start | bytes 12292
Sparse Core Ops, SparseCore 0:
  36.7 34.2 all-gather.1
  85.2 34.2 reduce-scatter.1
where the time goes:
time: 151 us
  waiting for transfers between devices  76.1 us (50%)
  blocking collectives  33.6 us (22%)
  matrix products  14 us (9%)
  between operations  13.5 us (9%)
  other arithmetic  8.29 us (5%)
  starting transfers between devices  3.5 us (2%)
  local copies, waits for them, and re-layouts  1.9 us (1%)
    reduce_scatter x1, waiting for transfers between devices, shards(): lax.psum_scatter(lax.dot_general(down_shard, hidden, (((0,), (1,)), ((),...  34.4 us
    all_gather x1, waiting for transfers between devices, shards(): lax.all_gather(incoming.reshape(-1, shard_width), 'tp', axis=1, tiled=True)  34.4 us
    psum x1, blocking collectives, shards(): square_sum = lax.psum(jnp.sum(resident * resident, axis=1), 'tp')  13.5 us
    all_to_all x1, blocking collectives, shards(): lax.all_to_all(outgoing, 'ep', split_axis=0, concat_axis=0, tiled=True)  10.5 us
    psum x1, blocking collectives, shards(): out_sum = lax.psum(jnp.sum(mixed_rows * mixed_rows, axis=1), 'tp')  9.64 us
    dot_general x1, matrix products, shards(): lax.dot_general(down_shard, hidden, (((0,), (1,)), ((), ())), preferred_e...  9.25 us
    all_to_all x1, waiting for transfers between devices, shards(): lax.all_to_all(expert_out, 'ep', split_axis=1, concat_axis=1, tiled=True)  7.26 us
    dot_general x1, matrix products, shards(): jnp.dot(picked_rows, expert_gate[0], preferred_element_type=jnp.float32)  4.76 us
  transfers between devices with their start and end apart: 3, of which 3 were waited for; matrix products, arithmetic and copies ran while one was open for 0% of the time, Pallas kernels for 0%

commit v1 on v0

--- a/solution.py
+++ b/solution.py
@@ -4,6 +4,21 @@
 from jax.sharding import PartitionSpec as P
 
 NORM_EPS = 1e-06
+
+
+def wait_threads(block_here, dim_at, mat):
+    p_next = block_here.shape
+    return jnp.moveaxis(
+        block_here.reshape(*p_next[:dim_at], mat, p_next[dim_at] // mat, *p_next[dim_at + 1 :]),
+        dim_at,
+        0,
+    )
+
+
+def _start_face(patch, dim_k):
+    back = list(patch.shape[1:])
+    back[dim_k] *= patch.shape[0]
+    return jnp.moveaxis(patch, 0, dim_k).reshape(back)
 
 
 def shards(tokens, pre_gain, out_gain, chosen, route_weight, expert_gate, expert_up, expert_down):
@@ -36,7 +51,16 @@
         tiled=True,
     )
     expert_out = summed.reshape(shard_width, experts_all, slot_count)
-    returned = lax.all_to_all(expert_out, "ep", split_axis=1, concat_axis=1, tiled=True)
+    top, carry_in = (lax.axis_size("ep"), lax.axis_index("ep"))
+    v1 = wait_threads(expert_out, 1, top)
+    runs = [v1[carry_in]]
+    for i in [*range(1, top)]:
+        local_part = v1[carry_in ^ i]
+        runs.append(
+            lax.ppermute(local_part, axis_name="ep", perm=[(it, it ^ i) for it in range(top)])
+        )
+    v1 = jnp.stack(runs, axis=0)[carry_in ^ jnp.arange(top)]
+    returned = _start_face(v1, 1)
     weighted = returned.astype(jnp.float32) * route_weight[0][None]
     flat_weighted = weighted.reshape(shard_width, experts_all * slot_count)
     update_cols = (

time: 151 us -> 150 us (level)
  waiting for transfers between devices: 76.1 us -> 73.4 us
  local copies, waits for them, and re-layouts: 1.9 us -> 4.26 us
  starting transfers between devices: 3.5 us -> 1.97 us
    all_to_all x1 -> x0, waiting for transfers between devices: 7.26 us -> none  [shards(): lax.all_to_all(expert_out, 'ep', split_axis=1, concat_axis=1, tiled=True)]
    ppermute x0 -> x3, waiting for transfers between devices: none -> 5.34 us  [shards(): lax.ppermute(local_part, axis_name='ep', perm=[(it, it ^ i) for it in ran...]
    all_to_all x1 -> x0, starting transfers between devices: 3.46 us -> none  [shards(): lax.all_to_all(expert_out, 'ep', split_axis=1, concat_axis=1, tiled=True)]
    ppermute x0 -> x3, starting transfers between devices: none -> 1.93 us  [shards(): lax.ppermute(local_part, axis_name='ep', perm=[(it, it ^ i) for it in ran...]
  transfers between devices with their start and end apart: 3 -> 5, of which waited for: 3 -> 4; matrix products, arithmetic and copies ran while one was open for 0% -> 0% of each run, Pallas kernels for 0% -> 0%
where the time goes in v1:
time: 150 us; the launch traced here: 149 us
  waiting for transfers between devices  73.4 us (49%)
  blocking collectives  33.6 us (22%)
  matrix products  14 us (9%)
  between operations  13.5 us (9%)
  other arithmetic  8.48 us (6%)
  local copies, waits for them, and re-layouts  4.26 us (3%)
  starting transfers between devices  1.97 us (1%)
    all_gather x1, waiting for transfers between devices, shards(): lax.all_gather(incoming.reshape(-1, shard_width), 'tp', axis=1, tiled=True)  34.4 us
    reduce_scatter x1, waiting for transfers between devices, shards(): lax.psum_scatter(lax.dot_general(down_shard, hidden, (((0,), (1,)), ((),...  33.6 us
    psum x1, blocking collectives, shards(): square_sum = lax.psum(jnp.sum(resident * resident, axis=1), 'tp')  13.5 us
    all_to_all x1, blocking collectives, shards(): lax.all_to_all(outgoing, 'ep', split_axis=0, concat_axis=0, tiled=True)  10.5 us
    psum x1, blocking collectives, shards(): out_sum = lax.psum(jnp.sum(mixed_rows * mixed_rows, axis=1), 'tp')  9.64 us
    dot_general x1, matrix products, shards(): lax.dot_general(down_shard, hidden, (((0,), (1,)), ((), ())), preferred_e...  9.25 us
    ppermute x3, waiting for transfers between devices, shards(): lax.ppermute(local_part, axis_name='ep', perm=[(it, it ^ i) for it in ran...  5.34 us
    dot_general x1, matrix products, shards(): jnp.dot(picked_rows, expert_gate[0], preferred_element_type=jnp.float32)  4.76 us
  transfers between devices with their start and end apart: 5, of which 4 were waited for; matrix products, arithmetic and copies ran while one was open for 0% of the time, Pallas kernels for 0%

profile of v1, /device:TPU:0, one launch (start us, length us, event | category | flops | bytes accessed | tf_op | source)
XLA Modules:
  0.0 149.2 jit_solution(679117225496469679)
XLA Ops:
  6.5 0.0 all-gather.2.cloned.1.call-start
  6.5 0.7 compare_select_fusion.1
  7.2 0.7 compare_and_fusion
  7.9 1.4 fusion.12
  9.3 13.5 %psum.14 = f32[384]{0:T(512)S(1)} all-reduce(f32[384]{0:T(512)S(1)} %fusion.12), channel_id=1, replica_groups=mesh['grp'=2,'ep'=4,'tp'=4] {'tp'}, use_global_device_ids=true, to_apply=%region_1.0 | all-reduce | flops 384 | bytes 3072 | tf_op jit(solution)/shard_map/psum | solution.py:32
  22.8 0.1 reshape.103
  22.9 0.7 dynamic_slice.4
  23.6 1.4 fusion.14
  24.9 1.0 gather_fusion
  26.0 0.1 broadcast_select_fusion
  26.1 10.5 %all_to_all.5 = bf16[4,48,1024]{2,1,0:T(8,128)(2,1)} all-to-all(bf16[4,48,1024]{2,1,0:T(8,128)(2,1)S(1)} %broadcast_select_fusion), channel_id=1, replica_groups=mesh['grp'=2,'ep'=4,'tp'=4] {'ep'}, dimensions={0} | all-to-all | bytes 786432 | tf_op jit(solution)/shard_map/all_to_all | solution.py:39
  36.5 0.0 all-gather.2.cloned.1.call-update
  36.6 0.0 reduce-scatter.2.cloned.1.call-start
  36.6 34.4 %all-gather.2.cloned.1.call-done = bf16[192,4096]{1,0:T(8,128)(2,1)} async-done(((bf16[192,1024]{1,0:T(8,128)(2,1)}), bf16[192,4096]{1,0:T(8,128)(2,1)}) %all-gather.2.cloned.1.call-update) | async-done | bytes 1572880 | tf_op jit(solution)/shard_map/all_gather | solution.py:40
  71.0 0.0 copy-start.4
  71.0 4.8 %fusion.4 = f32[192,768]{1,0:T(8,128)S(1)} fusion(bf16[192,4096]{1,0:T(8,128)(2,1)} %all-gather.2.cloned.1.call-done, bf16[1,4096,768]{2,1,0:T(8,128)(2,1)} %param.13), kind=kOutput, calls=%fused_computation.7 | convolution fusion | flops 1207959552 | bytes 8454144 | tf_op jit(solution)/shard_map/dot_general | solution.py:41
  75.8 0.0 copy-done.4
  75.8 9.3 %fusion.9 = bf16[4096,192]{0,1:T(8,128)(2,1)} fusion(bf16[1,768,4096]{2,1,0:T(8,128)(2,1)} %param.15, bf16[192,4096]{1,0:T(8,128)(2,1)S(1)} %copy-done.4, bf16[1,4096,768]{2,1,0:T(8,128)(2,1)} %param.14, f32[192,768]{1,0:T(8,128)S(1)} %fusion.4), kind=kOutput, calls=%fused_computation.10 | convolution fusion | flops 2417590272 | bytes 16318464 | tf_op jit(solution)/shard_map/dot_general | solution.py:46
  85.0 0.0 copy-start.1
  85.0 0.0 copy-start.3
  85.0 0.0 reduce-scatter.2.cloned.1.call-update
  85.1 0.7 copy-done.1
  85.7 0.1 reshape_squeeze.3
  85.8 0.0 copy-done.3
  85.8 0.1 mul.67
  85.9 33.6 %reduce-scatter.2.cloned.1.call-done = bf16[1024,192]{0,1:T(8,128)(2,1)} async-done(((bf16[4096,192]{0,1:T(8,128)(2,1)}), bf16[1024,192]{0,1:T(8,128)(2,1)}) %reduce-scatter.2.cloned.1.call-update) | async-done | bytes 393232 | tf_op jit(solution)/shard_map/reduce_scatter | solution.py:45
  119.5 1.1 dynamic-slice_bitcast_fusion.3
  120.6 0.6 collective-permute-start.2
  121.2 1.0 collective-permute-start.1
  122.2 0.3 collective-permute-start
  122.5 3.2 %collective-permute-done.2 = bf16[1024,1,48]{0,2,1:T(8,128)(2,1)S(1)} collective-permute-done((bf16[1024,1,48]{0,2,1:T(8,128)(2,1)S(1)}, bf16[1024,1,48]{0,2,1:T(8,128)(2,1)S(1)}, u32[]{:S(2)}, u32[]{:S(2)}) %collective-permute-start.2) | collective-permute-done | bytes 98336 | tf_op jit(solution)/shard_map/ppermute | solution.py:60
  125.7 2.1 %collective-permute-done.1 = bf16[1024,1,48]{0,2,1:T(8,128)(2,1)S(1)} collective-permute-done((bf16[1024,1,48]{0,2,1:T(8,128)(2,1)S(1)}, bf16[1024,1,48]{0,2,1:T(8,128)(2,1)S(1)}, u32[]{:S(2)}, u32[]{:S(2)}) %collective-permute-start.1) | collective-permute-done | bytes 98336 | tf_op jit(solution)/shard_map/ppermute | solution.py:60
  127.8 0.0 collective-permute-done
  127.8 0.1 maximum_bitcast_fusion
  127.9 0.6 gather_fusion.1
  128.5 0.1 bitcast_convert_fusion
  128.6 0.1 bitcast_multiply_fusion
  128.7 0.0 copy-start
  128.7 2.5 %scatter_custom_fusion = f32[1024,384]{0,1:T(8,128)S(1)} fusion(s32[192]{0:T(256)S(1)} %bitcast.72, f32[1024,192]{0,1:T(8,128)S(1)} %bitcast_multiply_fusion, f32[]{:T(128)} %constant.16.clone.1), kind=kCustom, calls=%fused_computation.22 | custom fusion | flops 196608 | bytes 2359300 | tf_op jit(solution)/shard_map/scatter-add | solution.py:69
  131.2 0.0 copy-done
  131.3 0.0 copy-start.2
  131.3 0.3 multiply_reduce_fusion
  131.6 9.6 %psum.15 = f32[384]{0:T(512)S(1)} all-reduce(f32[384]{0:T(512)S(1)} %multiply_reduce_fusion), channel_id=1, replica_groups=mesh['grp'=2,'ep'=4,'tp'=4] {'tp'}, use_global_device_ids=true, to_apply=%region_5.6 | all-reduce | flops 384 | bytes 3072 | tf_op jit(solution)/shard_map/psum | solution.py:72
  141.2 0.0 copy-done.2
  141.2 1.1 multiply_convert_fusion
  (6 shorter events, 0.0 us)
Async XLA Ops:
  6.5 64.5 %all-gather.2.cloned.1.call-start = ((), (), s32[]{:S(2)}) async-start(), calls=%async_computation.2 | async-start | bytes 1966080 | tf_op jit(solution)/shard_map/all_gather | solution.py:40
  36.6 82.9 %reduce-scatter.2.cloned.1.call-start = ((), (), s32[]{:S(2)}) async-start(), calls=%async_computation.3 | async-start | bytes 1966080 | tf_op jit(solution)/shard_map/reduce_scatter | solution.py:45
  71.0 4.8 %copy-start.4 = (bf16[192,4096]{1,0:T(8,128)(2,1)S(1)}, bf16[192,4096]{1,0:T(8,128)(2,1)}, u32[]{:S(2)}) copy-start(bf16[192,4096]{1,0:T(8,128)(2,1)} %all-gather.2.cloned.1.call-done) | copy-start | bytes 4718596
  85.0 0.7 copy-start.1
  85.0 0.8 copy-start.3
  120.6 5.1 %collective-permute-start.2 = (bf16[1024,1,48]{0,2,1:T(8,128)(2,1)S(1)}, bf16[1024,1,48]{0,2,1:T(8,128)(2,1)S(1)}, u32[]{:S(2)}, u32[]{:S(2)}) collective-permute-start(bf16[1024,1,48]{0,2,1:T(8,128)(2,1)S(1)} %get-tuple-element.6), channel_id=1, source_target_pairs={{0,12},{4,8},{8,4},{12,0},{1,13},{5,9},{9,5},{13,1},{2,14},{6,10},... | collective-permute-start | bytes 294920 | tf_op jit(solution)/shard_map/ppermute | solution.py:60
  121.2 6.7 %collective-permute-start.1 = (bf16[1024,1,48]{0,2,1:T(8,128)(2,1)S(1)}, bf16[1024,1,48]{0,2,1:T(8,128)(2,1)S(1)}, u32[]{:S(2)}, u32[]{:S(2)}) collective-permute-start(bf16[1024,1,48]{0,2,1:T(8,128)(2,1)S(1)} %get-tuple-element.7), channel_id=1, source_target_pairs={{0,8},{4,12},{8,0},{12,4},{1,9},{5,13},{9,1},{13,5},{2,10},{6,14},... | collective-permute-start | bytes 294920 | tf_op jit(solution)/shard_map/ppermute | solution.py:60
  122.2 5.7 %collective-permute-start = (bf16[1024,1,48]{0,2,1:T(8,128)(2,1)S(1)}, bf16[1024,1,48]{0,2,1:T(8,128)(2,1)S(1)}, u32[]{:S(2)}, u32[]{:S(2)}) collective-permute-start(bf16[1024,1,48]{0,2,1:T(8,128)(2,1)S(1)} %get-tuple-element.8), channel_id=1, source_target_pairs={{0,4},{4,0},{8,12},{12,8},{1,5},{5,1},{9,13},{13,9},{2,6},{6,2},{1... | collective-permute-start | bytes 294920 | tf_op jit(solution)/shard_map/ppermute | solution.py:60
  128.7 2.6 %copy-start = (bf16[384,1024]{1,0:T(8,128)(2,1)S(1)}, bf16[384,1024]{1,0:T(8,128)(2,1)}, u32[]{:S(2)}) copy-start(bf16[384,1024]{1,0:T(8,128)(2,1)} %param.8) | copy-start | bytes 2359300
  131.3 9.9 %copy-start.2 = (f32[1024]{0:T(1024)S(1)}, f32[1024]{0:T(1024)}, u32[]{:S(2)}) copy-start(f32[1024]{0:T(1024)} %param.10) | copy-start | bytes 12292
Sparse Core Ops, SparseCore 0:
  36.7 34.2 all-gather.1
  85.2 34.2 reduce-scatter.1
